TPU v7x, 32 devices: a whole 2x2x4 slice. The times are simulated.
32 devices in a mesh: ep: 8 (over z, y), tp: 4 (over x, core).
Axes of the slice: x: 2, y: 2, z: 4, core: 2. Of those that a mesh axis runs over, the one named last changes fastest.
Arguments:
- tokens: bfloat16 [192, 2048], P('ep'), may hold values from -6 to 6
- delta_state: float32 [192, 8, 128, 128], P('ep', 'tp'), may hold values from -3 to 3
- first_gain: bfloat16 [2048], replicated, may hold values from 0.099609375 to 1.8984375
- query_weight: bfloat16 [2048, 1024], P(None, 'tp'), may hold values from -0.125 to 0.125
- key_weight: bfloat16 [2048, 1024], P(None, 'tp'), may hold values from -0.125 to 0.125
- value_weight: bfloat16 [2048, 1024], P(None, 'tp'), may hold values from -0.125 to 0.125
- outgate_weight: bfloat16 [2048, 1024], P(None, 'tp'), may hold values from -0.125 to 0.125
- beta_weight: bfloat16 [2048, 8], replicated, may hold values from -0.125 to 0.125
- decay_weight: bfloat16 [2048, 8], replicated, may hold values from -0.125 to 0.125
- decay_rate: float32 [8], replicated, may hold values from 0.05 to 4
- decay_bias: float32 [8], replicated, may hold values from -3 to 3
- head_gain: bfloat16 [128], replicated, may hold values from 0.099609375 to 1.8984375
- out_weight: bfloat16 [1024, 2048], P('tp'), may hold values from -0.1875 to 0.1875
- second_gain: bfloat16 [2048], replicated, may hold values from 0.099609375 to 1.8984375
- blend_weight: bfloat16 [2048], replicated, may hold values from -0.125 to 0.125
- dense_gate_weight: bfloat16 [2048, 2048], P(None, 'tp'), may hold values from -0.125 to 0.125
- dense_up_weight: bfloat16 [2048, 2048], P(None, 'tp'), may hold values from -0.125 to 0.125
- dense_down_weight: bfloat16 [2048, 2048], P('tp'), may hold values from -0.125 to 0.125
- expert_gate: bfloat16 [32, 2048, 512], P(('ep', 'tp')), may hold values from -0.125 to 0.125
- expert_up: bfloat16 [32, 2048, 512], P(('ep', 'tp')), may hold values from -0.125 to 0.125
- expert_down: bfloat16 [32, 512, 2048], P(('ep', 'tp')), may hold values from -0.25 to 0.25
- route_ids: int32 [192, 6], P('ep'), may hold values from 0 to 31, all different within a row; in each aligned block of 24 rows (0 to 23, 24 to 47, ...) at most 7 rows name the same one
- route_weights: float32 [192, 6], P('ep'), may hold values from 0.1 to 1
Outputs:
- new_tokens: bfloat16 [192, 2048], P('ep')
- new_state: float32 [192, 8, 128, 128], P('ep', 'tp')
Inputs may be any that keep to these rules, and one draw needn't show every extreme that they name: `route_ids`: each row names 6 different experts. In each aligned block of 24 rows (the sequences of one index of ep) no expert is named by more than 7 rows, and in some block an expert is named by exactly 7 rows.
All inputs are finite; a program needn't handle non-finite values.
Results may differ from a plain program's by a relative error of at most 0.017.
Values may be sent and summed in bfloat16 or wider, within the bound.
A program may use at most 128 MiB of HBM per device.

v0:
```python
import jax
import jax.numpy as jnp
from jax import lax
from jax.sharding import PartitionSpec as P

norm_eps = 1e-06
unit_eps = 1e-06
routed_scale = 2.5


def rms_scale(values, gain):
    values = values.astype(jnp.float32)
    inverse = lax.rsqrt(jnp.mean(values * values, axis=-1, keepdims=True) + norm_eps)
    return values * inverse * gain.astype(jnp.float32)


def unit_rows(values):
    return values * lax.rsqrt(jnp.sum(values * values, axis=-1, keepdims=True) + unit_eps)


def rounded(values):
    return lax.optimization_barrier(values.astype(jnp.bfloat16)).astype(jnp.float32)


def delta_update(delta_state, query_raw, key_raw, value_raw, beta_gate, log_decay):
    head_size = delta_state.shape[-1]
    query_unit = unit_rows(jax.nn.silu(query_raw)) * head_size ** (-0.5)
    key_unit = unit_rows(jax.nn.silu(key_raw))
    value_act = jax.nn.silu(value_raw)
    decayed = jnp.exp(log_decay)[:, :, None, None] * delta_state
    predicted = jnp.einsum("shkv,shk->shv", decayed, key_unit, precision=lax.Precision.HIGHEST)
    update = (beta_gate[:, :, None] * key_unit)[:, :, :, None] * (value_act - predicted)[
        :, :, None, :
    ]
    new_state = decayed + update
    readout = jnp.einsum("shkv,shk->shv", new_state, query_unit, precision=lax.Precision.HIGHEST)
    return (new_state, readout)


def gated_heads(readout, outgate_raw, head_gain):
    scaled = rms_scale(readout, head_gain) * jax.nn.silu(outgate_raw)
    return scaled.reshape(scaled.shape[0], -1).astype(jnp.bfloat16)


def expert_rows(row_block, gate_mat, up_mat, down_mat):
    gate_part = jnp.dot(row_block, gate_mat, preferred_element_type=jnp.float32)
    up_part = jnp.dot(row_block, up_mat, preferred_element_type=jnp.float32)
    hidden = (jax.nn.silu(gate_part) * up_part).astype(jnp.bfloat16)
    return jnp.dot(hidden, down_mat, preferred_element_type=jnp.float32).astype(jnp.bfloat16)


def shards(
    tokens,
    delta_state,
    first_gain,
    query_weight,
    key_weight,
    value_weight,
    outgate_weight,
    beta_weight,
    decay_weight,
    decay_rate,
    decay_bias,
    head_gain,
    out_weight,
    second_gain,
    blend_weight,
    dense_gate_weight,
    dense_up_weight,
    dense_down_weight,
    expert_gate,
    expert_up,
    expert_down,
    route_ids,
    route_weights,
):
    seq_count = tokens.shape[0]
    head_local = delta_state.shape[1]
    head_size = delta_state.shape[2]
    top_count = route_ids.shape[1]
    ep_count = lax.axis_size("ep")
    tp_count = lax.axis_size("tp")
    tp_index = lax.axis_index("tp")
    normed = rms_scale(tokens, first_gain).astype(jnp.bfloat16)

    def project(weight):
        product = jnp.dot(normed, weight, preferred_element_type=jnp.float32)
        return rounded(product).reshape(seq_count, head_local, head_size)

    query_raw = project(query_weight)
    key_raw = project(key_weight)
    value_raw = project(value_weight)
    outgate_raw = project(outgate_weight)
    head_start = tp_index * head_local
    beta_all = jax.nn.sigmoid(jnp.dot(normed, beta_weight, preferred_element_type=jnp.float32))
    beta_gate = lax.dynamic_slice_in_dim(beta_all, head_start, head_local, 1)
    decay_input = jnp.dot(normed, decay_weight, preferred_element_type=jnp.float32) + decay_bias
    decay_all = -decay_rate * jax.nn.softplus(decay_input)
    log_decay = lax.dynamic_slice_in_dim(decay_all, head_start, head_local, 1)
    new_state, readout = delta_update(
        delta_state, query_raw, key_raw, value_raw, beta_gate, log_decay
    )
    gated = gated_heads(readout, outgate_raw, head_gain)
    mix_part = jnp.dot(gated, out_weight, preferred_element_type=jnp.float32)
    row_local = seq_count // tp_count
    mixed_rows = lax.psum_scatter(
        mix_part.astype(jnp.bfloat16), "tp", scatter_dimension=0, tiled=True
    ).astype(jnp.float32)
    own_tokens = lax.dynamic_slice_in_dim(tokens, tp_index * row_local, row_local, 0)
    residual_rows = (own_tokens.astype(jnp.float32) + mixed_rows).astype(jnp.bfloat16)
    normed_rows = rms_scale(residual_rows, second_gain).astype(jnp.bfloat16)
    normed_mid, residual = (
        lax.all_gather(normed_rows, "tp", axis=0, tiled=True),
        lax.all_gather(residual_rows, "tp", axis=0, tiled=True),
    )
    blend_gate = jax.nn.sigmoid(
        jnp.dot(normed_mid, blend_weight, preferred_element_type=jnp.float32)
    )
    dense_gate_raw = jnp.dot(normed_mid, dense_gate_weight, preferred_element_type=jnp.float32)
    dense_up_raw = jnp.dot(normed_mid, dense_up_weight, preferred_element_type=jnp.float32)
    dense_hidden = (jax.nn.silu(dense_gate_raw) * dense_up_raw).astype(jnp.bfloat16)
    dense_part = jnp.dot(dense_hidden, dense_down_weight, preferred_element_type=jnp.float32)
    expert_count = ep_count * tp_count
    capacity = max(2, (3 * seq_count * top_count + 2 * expert_count - 1) // (2 * expert_count))
    flat_ids = route_ids.reshape(-1)
    assign_count = flat_ids.shape[0]
    earlier = jnp.arange(assign_count)[:, None] > jnp.arange(assign_count)[None, :]
    matches = (flat_ids[:, None] == flat_ids[None, :]) & earlier
    rank_of = jnp.sum(matches.astype(jnp.int32), axis=1)
    owned = flat_ids % tp_count == tp_index
    slot_of = jnp.where(owned, flat_ids // tp_count * capacity + rank_of, -1)
    slot_total = ep_count * capacity
    slot_grid = slot_of.reshape(seq_count, top_count)
    slot_range = jnp.arange(slot_total, dtype=jnp.int32)
    dispatch = jnp.any(slot_grid[None, :, :] == slot_range[:, None, None], axis=2).astype(
        jnp.bfloat16
    )
    model_width = normed_mid.shape[1]
    outgoing = jnp.dot(dispatch, normed_mid, preferred_element_type=jnp.float32).astype(
        jnp.bfloat16
    )
    outgoing = outgoing.reshape(ep_count, capacity, model_width)
    arrived = lax.all_to_all(outgoing, "ep", split_axis=0, concat_axis=0, tiled=True)
    result = expert_rows(
        arrived.reshape(-1, model_width), expert_gate[0], expert_up[0], expert_down[0]
    )
    returned = lax.all_to_all(
        result.reshape(arrived.shape), "ep", split_axis=0, concat_axis=0, tiled=True
    )
    returned_rows = returned.reshape(slot_total, model_width)
    picked = returned_rows[jnp.maximum(slot_of, 0)].astype(jnp.float32)
    picked = picked.reshape(seq_count, top_count, model_width)
    route_scale = route_weights / jnp.sum(route_weights, axis=1, keepdims=True) * routed_scale
    kept_scale = jnp.where(owned.reshape(seq_count, top_count), route_scale, 0.0)
    routed_part = jnp.sum(kept_scale[:, :, None] * picked, axis=1)
    combined = lax.psum(
        (routed_part + blend_gate[:, None] * dense_part).astype(jnp.bfloat16), "tp"
    ).astype(jnp.float32)
    new_tokens = (residual.astype(jnp.float32) + combined).astype(jnp.bfloat16)
    return (new_tokens, new_state)


def solution(mesh):
    placed = (
        P("ep", None),
        P("ep", "tp", None, None),
        P(),
        P(None, "tp"),
        P(None, "tp"),
        P(None, "tp"),
        P(None, "tp"),
        P(),
        P(),
        P(),
        P(),
        P(),
        P("tp", None),
        P(),
        P(),
        P(None, "tp"),
        P(None, "tp"),
        P("tp", None),
        P(("ep", "tp"), None, None),
        P(("ep", "tp"), None, None),
        P(("ep", "tp"), None, None),
        P("ep", None),
        P("ep", None),
    )
    return jax.shard_map(
        shards,
        mesh=mesh,
        in_specs=placed,
        out_specs=(P("ep", None), P("ep", "tp", None, None)),
        check_vma=False,
    )
```

profile of v0, /device:TPU:0, one launch (start us, length us, event | category | flops | bytes accessed | tf_op | source)
XLA Modules:
  0.0 129.9 jit_solution(16252030878266203387)
XLA Ops:
  7.2 0.8 convert_element_type.92
  8.0 1.1 fusion.27
  9.1 0.7 neg.38
  9.8 1.1 fusion.22
  10.9 1.2 fusion.59
  12.2 1.6 %convolution_convert_fusion.6 = bf16[24,256]{1,0:T(8,128)(2,1)S(1)} fusion(bf16[2048,256]{1,0:T(8,128)(2,1)} %param.27, bf16[24,2048]{1,0:T(8,128)(2,1)} %param.23, f32[2048]{0:T(1024)S(1)} %convert_element_type.92, f32[24]{0:T(128)S(1)} %add_rsqrt_fusion.4), kind=kOutput, calls=%fused_computation.24 | convolution fusion | flops 25368576 | bytes 1167456 | tf_op jit(solution)/shard_map/dot_general | solution.py:87
  13.8 0.1 multiply_reduce_fusion.3
  14.0 1.6 %convolution_convert_fusion.5 = bf16[24,256]{1,0:T(8,128)(2,1)S(1)} fusion(bf16[2048,256]{1,0:T(8,128)(2,1)} %param.28, bf16[24,2048]{1,0:T(8,128)(2,1)} %param.23, f32[2048]{0:T(1024)S(1)} %convert_element_type.92, f32[24]{0:T(128)S(1)} %add_rsqrt_fusion.4), kind=kOutput, calls=%fused_computation.23 | convolution fusion | flops 25368576 | bytes 1167456 | tf_op jit(solution)/shard_map/dot_general | solution.py:87
  15.6 0.3 convolution_convert_fusion.4
  16.0 0.1 multiply_reduce_fusion.2
  16.1 0.1 broadcast_multiply_fusion.1
  16.2 4.9 %fusion.1 = f32[24,2,1,128]{3,2,1,0:T(1,128)S(1)} fusion(f32[24,2,128,1]{2,3,1,0:T(1,128)S(1)} %bitcast.71, f32[24,2,128,128]{3,2,1,0:T(8,128)} %param.24, f32[24,2]{1,0:T(8,128)S(1)} %copy.47), kind=kOutput, calls=%fused_computation.2 | convolution fusion | flops 10223616 | bytes 3195072 | tf_op jit(solution)/shard_map/shkv,shk->shv/dot_general | solution.py:31
  21.2 1.1 multiply_add_fusion
  22.5 1.5 %copy-done.2 = f32[24,2,128,128]{3,2,1,0:T(8,128)} copy-done((f32[24,2,128,128]{3,2,1,0:T(8,128)}, f32[24,2,128,128]{3,2,1,0:T(8,128)S(1)}, u32[]{:S(2)}) %copy-start.2) | copy-done | bytes 3145752
  24.0 2.8 %fusion.69 = f32[24,2,1,128]{3,2,1,0:T(1,128)S(1)} fusion(f32[24,2,128,128]{3,2,1,0:T(8,128)S(1)} %multiply_add_fusion, f32[24,2,128,1]{2,3,1,0:T(1,128)S(1)} %bitcast.73), kind=kOutput, calls=%fused_computation.112 | convolution fusion | flops 9437184 | bytes 3194880 | tf_op jit(solution)/shard_map/shkv,shk->shv/dot_general | solution.py:36
  26.8 0.1 multiply_reduce_fusion.1
  26.9 0.3 convolution_convert_fusion.3
  27.3 0.1 fusion.50
  27.4 0.2 convolution_convert_fusion.2
  27.6 9.7 %fusion = bf16[8,2048]{1,0:T(8,128)(2,1)S(1)} fusion(bf16[24,2048]{1,0:T(8,128)(2,1)S(1)} %convolution_convert_fusion.2), kind=kCustom, calls=%all-reduce-scatter | all-reduce-scatter fusion | flops 65537 | bytes 131584
  37.3 1.3 collective-permute-start
  38.7 0.1 eq.52
  38.8 0.2 convert_reduce_fusion
  39.0 0.1 reduce_sum.82
  39.2 0.1 fusion.36
  39.5 0.6 dynamic-slice.4
  40.7 0.2 concatenate
  40.9 0.2 fusion.37
  41.1 7.0 %all-gather.1 = bf16[4,6,2048]{2,1,0:T(8,128)(2,1)S(1)} all-gather(bf16[1,6,2048]{2,1,0:T(8,128)(2,1)S(1)} %fusion.46), channel_id=1, replica_groups=mesh['ep'=8,'tp'=4] {'tp'}, dimensions={0}, use_global_device_ids=true | all-gather | bytes 122880 | tf_op jit(solution)/shard_map/all_gather | solution.py:113
  48.1 0.3 convolution_convert_fusion.1
  48.4 0.8 reshape.269
  49.2 5.8 %all-to-all-start = ((bf16[8,7,2048]{2,1,0:T(8,128)(2,1)}), bf16[8,7,2048]{2,1,0:T(8,128)(2,1)S(1)}, u32[]{:S(2)}, u32[]{:S(2)}) async-start(bf16[8,7,2048]{2,1,0:T(8,128)(2,1)} %reshape.269), calls=%async_computation | async-start | bytes 524288 | tf_op jit(solution)/shard_map/all_to_all | solution.py:143
  55.2 9.2 %all-to-all-done = bf16[8,7,2048]{2,1,0:T(8,128)(2,1)S(1)} async-done(((bf16[8,7,2048]{2,1,0:T(8,128)(2,1)}), bf16[8,7,2048]{2,1,0:T(8,128)(2,1)S(1)}, u32[]{:S(2)}, u32[]{:S(2)}) %all-to-all-start) | async-done | bytes 229408 | tf_op jit(solution)/shard_map/all_to_all | solution.py:143
  64.5 2.0 %fusion.8 = f32[56,512]{1,0:T(8,128)S(1)} fusion(bf16[56,2048]{1,0:T(8,128)(2,1)S(1)} %reshape.270, bf16[1,2048,512]{2,1,0:T(8,128)(2,1)} %param.41), kind=kOutput, calls=%fused_computation.13 | convolution fusion | flops 117440512 | bytes 2441216 | tf_op jit(solution)/shard_map/dot_general | solution.py:46
  66.6 2.5 %convolution_convert_fusion = bf16[56,2048]{1,0:T(8,128)(2,1)S(1)} fusion(bf16[1,512,2048]{2,1,0:T(8,128)(2,1)S(1)} %copy-done, bf16[56,2048]{1,0:T(8,128)(2,1)S(1)} %reshape.270, bf16[1,2048,512]{2,1,0:T(8,128)(2,1)} %param.42, f32[56,512]{1,0:T(8,128)S(1)} %fusion.8), kind=kOutput, calls=%fused_computation.4 | convolution fusion | flops 235167744 | bytes 4767744 | tf_op jit(solution)/shard_map/dot_general | solution.py:49
  69.1 0.8 reshape.271
  69.8 3.6 %all-to-all-start.1 = ((bf16[8,7,2048]{2,1,0:T(8,128)(2,1)}), bf16[8,7,2048]{2,1,0:T(8,128)(2,1)S(1)}, u32[]{:S(2)}, u32[]{:S(2)}) async-start(bf16[8,7,2048]{2,1,0:T(8,128)(2,1)} %reshape.271), calls=%async_computation.1 | async-start | bytes 524288 | tf_op jit(solution)/shard_map/all_to_all | solution.py:147
  73.4 0.2 all-reduce.4.cloned.1.call-start
  73.6 0.1 fusion.26
  73.8 2.0 %fusion.70 = f32[24,512]{1,0:T(8,128)S(1)} fusion(bf16[24,2048]{1,0:T(8,128)(2,1)S(1)} %reshape.294, bf16[2048,512]{1,0:T(8,128)(2,1)} %param.38), kind=kOutput, calls=%fused_computation.113 | convolution fusion | flops 50331648 | bytes 2244608 | tf_op jit(solution)/shard_map/dot_general | solution.py:119
  75.8 6.6 %all-to-all-done.1 = bf16[8,7,2048]{2,1,0:T(8,128)(2,1)S(1)} async-done(((bf16[8,7,2048]{2,1,0:T(8,128)(2,1)}), bf16[8,7,2048]{2,1,0:T(8,128)(2,1)S(1)}, u32[]{:S(2)}, u32[]{:S(2)}) %all-to-all-start.1) | async-done | bytes 229408 | tf_op jit(solution)/shard_map/all_to_all | solution.py:147
  82.5 1.0 gather_fusion
  83.5 1.3 %reshape.282 = f32[24,6,2048]{2,1,0:T(8,128)} reshape(bf16[144,2048]{1,0:T(8,128)(2,1)S(1)} %gather_fusion) | data formatting | bytes 1769472 | tf_op jit(solution)/shard_map/convert_element_type | solution.py:151
  84.8 2.0 %multiply_reduce_fusion = f32[24,2048]{1,0:T(8,128)S(1)} fusion(f32[24,6,2048]{2,1,0:T(8,128)} %reshape.282, f32[24,6]{1,0:T(8,128)S(1)} %multiply_select_fusion), kind=kLoop, calls=%fused_computation.15 | loop fusion | flops 540672 | bytes 1376832 | tf_op jit(solution)/shard_map/reduce_sum | solution.py:155
  86.8 3.6 %fusion.4 = bf16[24,2048]{1,0:T(8,128)(2,1)} fusion(f32[24,2048]{1,0:T(8,128)S(1)} %multiply_reduce_fusion, bf16[512,2048]{1,0:T(8,128)(2,1)} %param.40, bf16[24,2048]{1,0:T(8,128)(2,1)S(1)} %reshape.294, bf16[2048,512]{1,0:T(8,128)(2,1)} %param.39, f32[24]{0:T(128)S(1)} %fusion.26, f32[24,512]{1,0:T(8,128)S(1)} %fusion.70), kind=kOutput, calls=%fused_computation.8 | convolution fusion | flops 100884480 | bytes 4636768 | tf_op jit(solution)/shard_map/dot_general | solution.py:122
  90.4 5.4 %all-gather = bf16[4,6,2048]{2,1,0:T(8,128)(2,1)S(1)} all-gather(bf16[1,6,2048]{2,1,0:T(8,128)(2,1)S(1)} %bitcast.68), channel_id=1, replica_groups=mesh['ep'=8,'tp'=4] {'tp'}, dimensions={0}, use_global_device_ids=true | all-gather | bytes 122880 | tf_op jit(solution)/shard_map/all_gather | solution.py:114
  95.9 25.7 %all-reduce.4.cloned.1.call-done = bf16[24,2048]{1,0:T(8,128)(2,1)} async-done(((bf16[24,2048]{1,0:T(8,128)(2,1)}), bf16[24,2048]{1,0:T(8,128)(2,1)}) %all-reduce.4.cloned.1.call-update) | async-done | bytes 98320 | tf_op jit(solution)/shard_map/psum | solution.py:156
  121.5 1.6 %add_convert_fusion = bf16[24,2048]{1,0:T(8,128)(2,1)} fusion(f32[24,2048]{1,0:T(8,128)S(1)} %reshape.295, bf16[24,2048]{1,0:T(8,128)(2,1)} %all-reduce.4.cloned.1.call-done), kind=kLoop, calls=%fused_computation.40 | loop fusion | flops 147456 | bytes 393216 | tf_op jit(solution)/shard_map/convert_element_type | solution.py:159
  (59 shorter events, 1.4 us)
Async XLA Ops:
  7.2 59.4 %copy-start = (bf16[1,512,2048]{2,1,0:T(8,128)(2,1)S(1)}, bf16[1,512,2048]{2,1,0:T(8,128)(2,1)}, u32[]{:S(2)}) copy-start(bf16[1,512,2048]{2,1,0:T(8,128)(2,1)} %param.43) | copy-start | bytes 6291460
  7.2 8.4 %copy-start.3 = (bf16[24,2048]{1,0:T(8,128)(2,1)S(1)}, bf16[24,2048]{1,0:T(8,128)(2,1)}, u32[]{:S(2)}) copy-start(bf16[24,2048]{1,0:T(8,128)(2,1)} %param.23) | copy-start | bytes 294916
  7.2 8.4 %copy-start.4 = (bf16[2048,256]{1,0:T(8,128)(2,1)S(1)}, bf16[2048,256]{1,0:T(8,128)(2,1)}, u32[]{:S(2)}) copy-start(bf16[2048,256]{1,0:T(8,128)(2,1)} %param.26) | copy-start | bytes 3145732
  16.0 5.3 %copy-start.1 = (f32[24,2,128,128]{3,2,1,0:T(8,128)S(1)}, f32[24,2,128,128]{3,2,1,0:T(8,128)}, u32[]{:S(2)}) copy-start(f32[24,2,128,128]{3,2,1,0:T(8,128)} %param.24) | copy-start | bytes 9437188
  22.3 1.7 %copy-start.2 = (f32[24,2,128,128]{3,2,1,0:T(8,128)}, f32[24,2,128,128]{3,2,1,0:T(8,128)S(1)}, u32[]{:S(2)}) copy-start(f32[24,2,128,128]{3,2,1,0:T(8,128)S(1)} %multiply_add_fusion) | copy-start | bytes 9437188
  22.4 4.6 %copy-start.5 = (bf16[2048,256]{1,0:T(8,128)(2,1)S(1)}, bf16[2048,256]{1,0:T(8,128)(2,1)}, u32[]{:S(2)}) copy-start(bf16[2048,256]{1,0:T(8,128)(2,1)} %param.29) | copy-start | bytes 3145732
  24.0 3.3 %copy-start.12 = (bf16[128]{0:T(256)(128)(2,1)S(1)}, bf16[128]{0:T(256)(128)(2,1)}, u32[]{:S(2)}) copy-start(bf16[128]{0:T(256)(128)(2,1)} %param.34) | copy-start | bytes 772
  24.0 3.4 %copy-start.6 = (bf16[256,2048]{1,0:T(8,128)(2,1)S(1)}, bf16[256,2048]{1,0:T(8,128)(2,1)}, u32[]{:S(2)}) copy-start(bf16[256,2048]{1,0:T(8,128)(2,1)} %param.35) | copy-start | bytes 3145732
  26.8 11.8 %copy-start.10 = (s32[24,6]{0,1:T(8,128)S(1)}, s32[24,6]{0,1:T(8,128)}, u32[]{:S(2)}) copy-start(s32[24,6]{0,1:T(8,128)} %param.44) | copy-start | bytes 1732
  26.8 12.6 %copy-start.8 = (bf16[2048]{0:T(1024)(128)(2,1)S(1)}, bf16[2048]{0:T(1024)(128)(2,1)}, u32[]{:S(2)}) copy-start(bf16[2048]{0:T(1024)(128)(2,1)} %param.36) | copy-start | bytes 12292
  26.8 12.7 %copy-start.11 = (u32[32]{0:T(128)S(1)}, u32[32]{0:T(128)}, u32[]{:S(2)}) copy-start(u32[32]{0:T(128)} %constant.90) | copy-start | bytes 388
  27.2 27.8 %copy-start.7 = (f32[24,6]{0,1:T(8,128)S(1)}, f32[24,6]{0,1:T(8,128)}, u32[]{:S(2)}) copy-start(f32[24,6]{0,1:T(8,128)} %param.45) | copy-start | bytes 1732
  27.2 27.9 %copy-start.9 = (bf16[2048]{0:T(1024)(128)(2,1)S(1)}, bf16[2048]{0:T(1024)(128)(2,1)}, u32[]{:S(2)}) copy-start(bf16[2048]{0:T(1024)(128)(2,1)} %param.37) | copy-start | bytes 12292
  37.3 3.4 %collective-permute-start = (bf16[6,2048]{1,0:T(8,128)(2,1)S(1)}, bf16[6,2048]{1,0:T(8,128)(2,1)S(1)}, u32[]{:S(2)}, u32[]{:S(2)}) collective-permute-start(bf16[6,2048]{1,0:T(8,128)(2,1)S(1)} %slice.2), channel_id=1, source_target_pairs={{0,1},{1,2},{2,3},{4,5},{5,6},{6,7},{8,9},{9,10},{10,11},{12,13},{... | collective-permute-start | bytes 73736
  49.2 15.3 %all-to-all-start = ((bf16[8,7,2048]{2,1,0:T(8,128)(2,1)}), bf16[8,7,2048]{2,1,0:T(8,128)(2,1)S(1)}, u32[]{:S(2)}, u32[]{:S(2)}) async-start(bf16[8,7,2048]{2,1,0:T(8,128)(2,1)} %reshape.269), calls=%async_computation | async-start | bytes 524288 | tf_op jit(solution)/shard_map/all_to_all | solution.py:143
  69.8 12.6 %all-to-all-start.1 = ((bf16[8,7,2048]{2,1,0:T(8,128)(2,1)}), bf16[8,7,2048]{2,1,0:T(8,128)(2,1)S(1)}, u32[]{:S(2)}, u32[]{:S(2)}) async-start(bf16[8,7,2048]{2,1,0:T(8,128)(2,1)} %reshape.271), calls=%async_computation.1 | async-start | bytes 524288 | tf_op jit(solution)/shard_map/all_to_all | solution.py:147
  73.4 48.1 %all-reduce.4.cloned.1.call-start = ((), (), s32[]{:S(2)}) async-start(), calls=%async_computation.2 | async-start | bytes 196608 | tf_op jit(solution)/shard_map/psum | solution.py:156
Sparse Core Ops, SparseCore 0:
  90.5 30.9 all-reduce.3
where the time goes:
time: 131 us; the launch traced here: 130 us
  waiting for transfers between devices  41.5 us (32%)
  matrix products  24.5 us (19%)
  blocking collectives  22 us (17%)
  between operations  15.1 us (12%)
  starting transfers between devices  10.9 us (8%)
  other arithmetic  8.59 us (7%)
  local copies, waits for them, and re-layouts  7.27 us (6%)
    psum x1, waiting for transfers between devices, shards(): lax.psum((routed_part + blend_gate[:, None] * dense_part).astype(jnp.bflo...  25.7 us
    unnamed x1, blocking collectives  9.66 us
    all_to_all x1, waiting for transfers between devices, shards(): lax.all_to_all(outgoing, 'ep', split_axis=0, concat_axis=0, tiled=True)  9.18 us
    all_gather x1, blocking collectives, shards(): lax.all_gather(normed_rows, 'tp', axis=0, tiled=True)  6.97 us
    all_to_all x1, waiting for transfers between devices, shards(): lax.all_to_all(result.reshape(arrived.shape), 'ep', split_axis=0, concat_...  6.63 us
    all_to_all x1, starting transfers between devices, shards(): lax.all_to_all(outgoing, 'ep', split_axis=0, concat_axis=0, tiled=True)  5.83 us
    all_gather x1, blocking collectives, shards(): lax.all_gather(residual_rows, 'tp', axis=0, tiled=True)  5.42 us
    dot_general x1, matrix products, delta_update(): jnp.einsum('shkv,shk->shv', decayed, key_unit, precision=lax.Precision.HI...  4.94 us
  transfers between devices with their start and end apart: 4, of which 3 were waited for; matrix products, arithmetic and copies ran while one was open for 3% of the time, Pallas kernels for 0%

commit v1 on v0

--- a/solution.py
+++ b/solution.py
@@ -1,3 +1,4 @@
+import functools
 import jax
 import jax.numpy as jnp
 from jax import lax
@@ -6,6 +7,13 @@
 norm_eps = 1e-06
 unit_eps = 1e-06
 routed_scale = 2.5
+
+
+def save_the_roads(sheet, mesh_ax):
+    return jax.lax.all_gather(sheet, axis_name=mesh_ax).sum(axis=0)
+
+
+_fix_block = functools.partial(save_the_roads, mesh_ax="tp")
 
 
 def rms_scale(values, gain):
@@ -153,8 +161,8 @@
     route_scale = route_weights / jnp.sum(route_weights, axis=1, keepdims=True) * routed_scale
     kept_scale = jnp.where(owned.reshape(seq_count, top_count), route_scale, 0.0)
     routed_part = jnp.sum(kept_scale[:, :, None] * picked, axis=1)
-    combined = lax.psum(
-        (routed_part + blend_gate[:, None] * dense_part).astype(jnp.bfloat16), "tp"
+    combined = _fix_block(
+        (routed_part + blend_gate[:, None] * dense_part).astype(jnp.bfloat16)
     ).astype(jnp.float32)
     new_tokens = (residual.astype(jnp.float32) + combined).astype(jnp.bfloat16)
     return (new_tokens, new_state)

time: 131 us -> 91.3 us (0.70)
  waiting for transfers between devices: 41.5 us -> 10.6 us
  between operations: 15.1 us -> 1.73 us
  blocking collectives: 22 us -> 28.7 us
    psum x1 -> x0, waiting for transfers between devices: 25.7 us -> none  [shards(): lax.psum((routed_part + blend_gate[:, None] * dense_part).astype(jnp.bflo...]
    all_gather x0 -> x1, blocking collectives: none -> 6.71 us  [save_the_roads(): return jax.lax.all_gather(sheet, axis_name=mesh_ax).sum(axis=0)]
    all_to_all x1, waiting for transfers between devices: 9.18 us -> 3.74 us  [shards(): lax.all_to_all(outgoing, 'ep', split_axis=0, concat_axis=0, tiled=True)]
  transfers between devices with their start and end apart: 4 -> 3, of which waited for: 3 -> 2; matrix products, arithmetic and copies ran while one was open for 3% -> 4% of each run, Pallas kernels for 0% -> 0%
where the time goes in v1:
time: 91.3 us; the launch traced here: 90.7 us
  blocking collectives  28.7 us (31%)
  matrix products  23.9 us (26%)
  starting transfers between devices  10.7 us (12%)
  waiting for transfers between devices  10.6 us (12%)
  other arithmetic  7.76 us (8%)
  local copies, waits for them, and re-layouts  7.27 us (8%)
  between operations  1.73 us (2%)
    unnamed x1, blocking collectives  9.66 us
    all_gather x1, blocking collectives, shards(): lax.all_gather(normed_rows, 'tp', axis=0, tiled=True)  6.97 us
    all_to_all x1, waiting for transfers between devices, shards(): lax.all_to_all(result.reshape(arrived.shape), 'ep', split_axis=0, concat_...  6.86 us
    all_gather x1, blocking collectives, save_the_roads(): return jax.lax.all_gather(sheet, axis_name=mesh_ax).sum(axis=0)  6.71 us
    all_to_all x1, starting transfers between devices, shards(): lax.all_to_all(outgoing, 'ep', split_axis=0, concat_axis=0, tiled=True)  5.83 us
    all_gather x1, blocking collectives, shards(): lax.all_gather(residual_rows, 'tp', axis=0, tiled=True)  5.4 us
    dot_general x1, matrix products, delta_update(): jnp.einsum('shkv,shk->shv', decayed, key_unit, precision=lax.Precision.HI...  4.94 us
    all_to_all x1, waiting for transfers between devices, shards(): lax.all_to_all(outgoing, 'ep', split_axis=0, concat_axis=0, tiled=True)  3.74 us
  transfers between devices with their start and end apart: 3, of which 2 were waited for; matrix products, arithmetic and copies ran while one was open for 4% of the time, Pallas kernels for 0%

profile of v1, /device:TPU:0, one launch (start us, length us, event | category | flops | bytes accessed | tf_op | source)
XLA Modules:
  0.0 90.7 jit_solution(17125129964318420340)
XLA Ops:
  0.7 0.8 convert_element_type.94
  1.5 1.1 %fusion.27 = f32[24]{0:T(128)S(1)} fusion(bf16[24,2048]{1,0:T(8,128)(2,1)} %param.23), kind=kLoop, calls=%fused_computation.37 | loop fusion | flops 147432 | bytes 98400 | tf_op jit(solution)/shard_map/reduce_sum | solution.py:21
  2.6 0.7 neg.38
  3.3 1.1 %fusion.22 = f32[24,8]{0,1:T(8,128)S(1)} fusion(bf16[2048,8]{0,1:T(8,128)(2,1)} %param.30, bf16[24,2048]{1,0:T(8,128)(2,1)} %param.23, f32[2048]{0:T(1024)S(1)} %convert_element_type.94, f32[24]{0:T(128)S(1)} %add_rsqrt_fusion.4), kind=kOutput, calls=%fused_computation.28 | convolution fusion | flops 983616 | bytes 140128 | tf_op jit(solution)/shard_map/dot_general | solution.py:103
  4.4 1.2 %fusion.59 = f32[24,8]{0,1:T(8,128)S(1)} fusion(bf16[2048,8]{0,1:T(8,128)(2,1)} %param.31, f32[8]{0:T(128)} %param.33, f32[8]{0:T(128)S(1)} %neg.38, bf16[24,2048]{1,0:T(8,128)(2,1)} %param.23, f32[2048]{0:T(1024)S(1)} %convert_element_type.94, f32[24]{0:T(128)S(1)} %add_rsqrt_fusion.4), kind=kOutput, calls=%fused_computation.97 | convolution fusion | flops 984576 | bytes 140192 | tf_op jit(solution)/shard_map/dot_general | solution.py:105
  5.6 1.6 %convolution_convert_fusion.6 = bf16[24,256]{1,0:T(8,128)(2,1)S(1)} fusion(bf16[2048,256]{1,0:T(8,128)(2,1)} %param.27, bf16[24,2048]{1,0:T(8,128)(2,1)} %param.23, f32[2048]{0:T(1024)S(1)} %convert_element_type.94, f32[24]{0:T(128)S(1)} %add_rsqrt_fusion.4), kind=kOutput, calls=%fused_computation.24 | convolution fusion | flops 25368576 | bytes 1167456 | tf_op jit(solution)/shard_map/dot_general | solution.py:95
  7.3 0.1 multiply_reduce_fusion.3
  7.5 1.6 %convolution_convert_fusion.5 = bf16[24,256]{1,0:T(8,128)(2,1)S(1)} fusion(bf16[2048,256]{1,0:T(8,128)(2,1)} %param.28, bf16[24,2048]{1,0:T(8,128)(2,1)} %param.23, f32[2048]{0:T(1024)S(1)} %convert_element_type.94, f32[24]{0:T(128)S(1)} %add_rsqrt_fusion.4), kind=kOutput, calls=%fused_computation.23 | convolution fusion | flops 25368576 | bytes 1167456 | tf_op jit(solution)/shard_map/dot_general | solution.py:95
  9.1 0.3 convolution_convert_fusion.4
  9.4 0.1 multiply_reduce_fusion.2
  9.6 0.1 broadcast_multiply_fusion.1
  9.7 4.9 %fusion.1 = f32[24,2,1,128]{3,2,1,0:T(1,128)S(1)} fusion(f32[24,2,128,1]{2,3,1,0:T(1,128)S(1)} %bitcast.73, f32[24,2,128,128]{3,2,1,0:T(8,128)} %param.24, f32[24,2]{1,0:T(8,128)S(1)} %copy.47), kind=kOutput, calls=%fused_computation.2 | convolution fusion | flops 10223616 | bytes 3195072 | tf_op jit(solution)/shard_map/shkv,shk->shv/dot_general | solution.py:39
  14.7 1.1 %multiply_add_fusion = f32[24,2,128,128]{3,2,1,0:T(8,128)S(1)} fusion(f32[24,2,128,128]{3,2,1,0:T(8,128)S(1)} %copy-done.1, f32[24,2,128]{2,1,0:T(2,128)S(1)} %fusion.47, f32[24,2,128]{2,1,0:T(2,128)S(1)} %get-tuple-element.6, f32[24,2]{1,0:T(8,128)S(1)} %copy.47), kind=kLoop, calls=%fused_computation.1 | loop fusion | flops 2359296 | bytes 6340800 | tf_op jit(solution)/shard_map/add | solution.py:43
  15.9 1.5 %copy-done.2 = f32[24,2,128,128]{3,2,1,0:T(8,128)} copy-done((f32[24,2,128,128]{3,2,1,0:T(8,128)}, f32[24,2,128,128]{3,2,1,0:T(8,128)S(1)}, u32[]{:S(2)}) %copy-start.2) | copy-done | bytes 3145752
  17.5 2.8 %fusion.69 = f32[24,2,1,128]{3,2,1,0:T(1,128)S(1)} fusion(f32[24,2,128,128]{3,2,1,0:T(8,128)S(1)} %multiply_add_fusion, f32[24,2,128,1]{2,3,1,0:T(1,128)S(1)} %bitcast.75), kind=kOutput, calls=%fused_computation.112 | convolution fusion | flops 9437184 | bytes 3194880 | tf_op jit(solution)/shard_map/shkv,shk->shv/dot_general | solution.py:44
  20.3 0.1 multiply_reduce_fusion.1
  20.4 0.3 convolution_convert_fusion.3
  20.7 0.1 fusion.50
  20.9 0.2 convolution_convert_fusion.2
  21.1 9.7 %fusion = bf16[8,2048]{1,0:T(8,128)(2,1)S(1)} fusion(bf16[24,2048]{1,0:T(8,128)(2,1)S(1)} %convolution_convert_fusion.2), kind=kCustom, calls=%all-reduce-scatter | all-reduce-scatter fusion | flops 65537 | bytes 131584
  30.8 1.3 %collective-permute-start = (bf16[6,2048]{1,0:T(8,128)(2,1)S(1)}, bf16[6,2048]{1,0:T(8,128)(2,1)S(1)}, u32[]{:S(2)}, u32[]{:S(2)}) collective-permute-start(bf16[6,2048]{1,0:T(8,128)(2,1)S(1)} %slice.2), channel_id=1, source_target_pairs={{0,1},{1,2},{2,3},{4,5},{5,6},{6,7},{8,9},{9,10},{10,11},{12,13},{... | collective-permute-start | bytes 73736
  32.2 0.1 eq.52
  32.3 0.2 convert_reduce_fusion
  32.5 0.1 reduce_sum.94
  32.7 0.1 fusion.36
  32.8 0.1 reshape.273
  32.9 0.6 dynamic-slice.4
  34.2 0.2 concatenate
  34.3 0.2 fusion.37
  34.6 7.0 %all-gather.2 = bf16[4,6,2048]{2,1,0:T(8,128)(2,1)S(1)} all-gather(bf16[1,6,2048]{2,1,0:T(8,128)(2,1)S(1)} %fusion.46), channel_id=1, replica_groups=mesh['ep'=8,'tp'=4] {'tp'}, dimensions={0}, use_global_device_ids=true | all-gather | bytes 122880 | tf_op jit(solution)/shard_map/all_gather | solution.py:121
  41.6 0.3 convolution_convert_fusion.1
  41.9 0.8 reshape.269
  42.6 5.8 %all-to-all-start = ((bf16[8,7,2048]{2,1,0:T(8,128)(2,1)}), bf16[8,7,2048]{2,1,0:T(8,128)(2,1)S(1)}, u32[]{:S(2)}, u32[]{:S(2)}) async-start(bf16[8,7,2048]{2,1,0:T(8,128)(2,1)} %reshape.269), calls=%async_computation | async-start | bytes 524288 | tf_op jit(solution)/shard_map/all_to_all | solution.py:151
  48.7 5.4 %all-gather.1 = bf16[4,6,2048]{2,1,0:T(8,128)(2,1)S(1)} all-gather(bf16[1,6,2048]{2,1,0:T(8,128)(2,1)S(1)} %bitcast.70), channel_id=1, replica_groups=mesh['ep'=8,'tp'=4] {'tp'}, dimensions={0}, use_global_device_ids=true | all-gather | bytes 122880 | tf_op jit(solution)/shard_map/all_gather | solution.py:122
  54.1 3.7 %all-to-all-done = bf16[8,7,2048]{2,1,0:T(8,128)(2,1)S(1)} async-done(((bf16[8,7,2048]{2,1,0:T(8,128)(2,1)}), bf16[8,7,2048]{2,1,0:T(8,128)(2,1)S(1)}, u32[]{:S(2)}, u32[]{:S(2)}) %all-to-all-start) | async-done | bytes 229408 | tf_op jit(solution)/shard_map/all_to_all | solution.py:151
  58.0 2.0 %fusion.8 = f32[56,512]{1,0:T(8,128)S(1)} fusion(bf16[56,2048]{1,0:T(8,128)(2,1)S(1)} %reshape.270, bf16[1,2048,512]{2,1,0:T(8,128)(2,1)} %param.41), kind=kOutput, calls=%fused_computation.13 | convolution fusion | flops 117440512 | bytes 2441216 | tf_op jit(solution)/shard_map/dot_general | solution.py:54
  60.0 2.5 %convolution_convert_fusion = bf16[56,2048]{1,0:T(8,128)(2,1)S(1)} fusion(bf16[1,512,2048]{2,1,0:T(8,128)(2,1)S(1)} %copy-done, bf16[56,2048]{1,0:T(8,128)(2,1)S(1)} %reshape.270, bf16[1,2048,512]{2,1,0:T(8,128)(2,1)} %param.42, f32[56,512]{1,0:T(8,128)S(1)} %fusion.8), kind=kOutput, calls=%fused_computation.4 | convolution fusion | flops 235167744 | bytes 4767744 | tf_op jit(solution)/shard_map/dot_general | solution.py:57
  62.5 0.8 reshape.271
  63.3 3.6 %all-to-all-start.1 = ((bf16[8,7,2048]{2,1,0:T(8,128)(2,1)}), bf16[8,7,2048]{2,1,0:T(8,128)(2,1)S(1)}, u32[]{:S(2)}, u32[]{:S(2)}) async-start(bf16[8,7,2048]{2,1,0:T(8,128)(2,1)} %reshape.271), calls=%async_computation.1 | async-start | bytes 524288 | tf_op jit(solution)/shard_map/all_to_all | solution.py:155
  66.9 0.1 fusion.26
  67.0 2.0 %fusion.70 = f32[24,512]{1,0:T(8,128)S(1)} fusion(bf16[24,2048]{1,0:T(8,128)(2,1)S(1)} %reshape.295, bf16[2048,512]{1,0:T(8,128)(2,1)} %param.38), kind=kOutput, calls=%fused_computation.113 | convolution fusion | flops 50331648 | bytes 2244608 | tf_op jit(solution)/shard_map/dot_general | solution.py:127
  69.0 6.9 %all-to-all-done.1 = bf16[8,7,2048]{2,1,0:T(8,128)(2,1)S(1)} async-done(((bf16[8,7,2048]{2,1,0:T(8,128)(2,1)}), bf16[8,7,2048]{2,1,0:T(8,128)(2,1)S(1)}, u32[]{:S(2)}, u32[]{:S(2)}) %all-to-all-start.1) | async-done | bytes 229408 | tf_op jit(solution)/shard_map/all_to_all | solution.py:155
  76.0 1.0 %gather_fusion = bf16[144,2048]{1,0:T(8,128)(2,1)S(1)} fusion(bf16[56,2048]{1,0:T(8,128)(2,1)S(1)} %reshape.272, s32[1024]{0:T(1024)S(1)} %pad_clamp_fusion), kind=kCustom, calls=%fused_computation | custom fusion | bytes 1180224 | tf_op jit(solution)/shard_map/gather | solution.py:159
  77.0 1.3 %reshape.282 = f32[24,6,2048]{2,1,0:T(8,128)} reshape(bf16[144,2048]{1,0:T(8,128)(2,1)S(1)} %gather_fusion) | data formatting | bytes 1769472 | tf_op jit(solution)/shard_map/convert_element_type | solution.py:159
  78.3 2.0 %multiply_reduce_fusion = f32[24,2048]{1,0:T(8,128)S(1)} fusion(f32[24,6,2048]{2,1,0:T(8,128)} %reshape.282, f32[24,6]{1,0:T(8,128)S(1)} %multiply_select_fusion), kind=kLoop, calls=%fused_computation.15 | loop fusion | flops 540672 | bytes 1376832 | tf_op jit(solution)/shard_map/reduce_sum | solution.py:163
  80.2 3.0 %fusion.4 = bf16[24,2048]{1,0:T(8,128)(2,1)S(1)} fusion(f32[24,2048]{1,0:T(8,128)S(1)} %multiply_reduce_fusion, bf16[512,2048]{1,0:T(8,128)(2,1)} %param.40, bf16[24,2048]{1,0:T(8,128)(2,1)S(1)} %reshape.295, bf16[2048,512]{1,0:T(8,128)(2,1)} %param.39, f32[24]{0:T(128)S(1)} %fusion.26, f32[24,512]{1,0:T(8,128)S(1)} %fusion.70), kind=kOutput, calls=%fused_computation.8 | convolution fusion | flops 100884480 | bytes 4636768 | tf_op jit(solution)/shard_map/dot_general | solution.py:130
  83.2 6.7 %all-gather = bf16[96,2048]{1,0:T(8,128)(2,1)S(1)} all-gather(bf16[24,2048]{1,0:T(8,128)(2,1)S(1)} %fusion.4), channel_id=2, replica_groups=mesh['ep'=8,'tp'=4] {'tp'}, dimensions={0}, use_global_device_ids=true | all-gather | bytes 491520 | tf_op jit(solution)/shard_map/all_gather | solution.py:13
  90.0 0.7 add_convert_fusion
  (58 shorter events, 1.3 us)
Async XLA Ops:
  0.6 59.4 %copy-start = (bf16[1,512,2048]{2,1,0:T(8,128)(2,1)S(1)}, bf16[1,512,2048]{2,1,0:T(8,128)(2,1)}, u32[]{:S(2)}) copy-start(bf16[1,512,2048]{2,1,0:T(8,128)(2,1)} %param.43) | copy-start | bytes 6291460
  0.6 8.4 %copy-start.3 = (bf16[24,2048]{1,0:T(8,128)(2,1)S(1)}, bf16[24,2048]{1,0:T(8,128)(2,1)}, u32[]{:S(2)}) copy-start(bf16[24,2048]{1,0:T(8,128)(2,1)} %param.23) | copy-start | bytes 294916
  0.7 8.4 %copy-start.4 = (bf16[2048,256]{1,0:T(8,128)(2,1)S(1)}, bf16[2048,256]{1,0:T(8,128)(2,1)}, u32[]{:S(2)}) copy-start(bf16[2048,256]{1,0:T(8,128)(2,1)} %param.26) | copy-start | bytes 3145732
  9.4 5.3 %copy-start.1 = (f32[24,2,128,128]{3,2,1,0:T(8,128)S(1)}, f32[24,2,128,128]{3,2,1,0:T(8,128)}, u32[]{:S(2)}) copy-start(f32[24,2,128,128]{3,2,1,0:T(8,128)} %param.24) | copy-start | bytes 9437188
  15.8 1.7 %copy-start.2 = (f32[24,2,128,128]{3,2,1,0:T(8,128)}, f32[24,2,128,128]{3,2,1,0:T(8,128)S(1)}, u32[]{:S(2)}) copy-start(f32[24,2,128,128]{3,2,1,0:T(8,128)S(1)} %multiply_add_fusion) | copy-start | bytes 9437188
  15.8 4.6 %copy-start.5 = (bf16[2048,256]{1,0:T(8,128)(2,1)S(1)}, bf16[2048,256]{1,0:T(8,128)(2,1)}, u32[]{:S(2)}) copy-start(bf16[2048,256]{1,0:T(8,128)(2,1)} %param.29) | copy-start | bytes 3145732
  17.5 3.3 %copy-start.12 = (bf16[128]{0:T(256)(128)(2,1)S(1)}, bf16[128]{0:T(256)(128)(2,1)}, u32[]{:S(2)}) copy-start(bf16[128]{0:T(256)(128)(2,1)} %param.34) | copy-start | bytes 772
  17.5 3.4 %copy-start.6 = (bf16[256,2048]{1,0:T(8,128)(2,1)S(1)}, bf16[256,2048]{1,0:T(8,128)(2,1)}, u32[]{:S(2)}) copy-start(bf16[256,2048]{1,0:T(8,128)(2,1)} %param.35) | copy-start | bytes 3145732
  20.2 11.8 %copy-start.10 = (s32[24,6]{0,1:T(8,128)S(1)}, s32[24,6]{0,1:T(8,128)}, u32[]{:S(2)}) copy-start(s32[24,6]{0,1:T(8,128)} %param.44) | copy-start | bytes 1732
  20.3 12.6 %copy-start.8 = (bf16[2048]{0:T(1024)(128)(2,1)S(1)}, bf16[2048]{0:T(1024)(128)(2,1)}, u32[]{:S(2)}) copy-start(bf16[2048]{0:T(1024)(128)(2,1)} %param.36) | copy-start | bytes 12292
  20.3 12.7 %copy-start.11 = (u32[32]{0:T(128)S(1)}, u32[32]{0:T(128)}, u32[]{:S(2)}) copy-start(u32[32]{0:T(128)} %constant.92) | copy-start | bytes 388
  20.7 27.8 %copy-start.7 = (f32[24,6]{0,1:T(8,128)S(1)}, f32[24,6]{0,1:T(8,128)}, u32[]{:S(2)}) copy-start(f32[24,6]{0,1:T(8,128)} %param.45) | copy-start | bytes 1732
  20.7 27.9 %copy-start.9 = (bf16[2048]{0:T(1024)(128)(2,1)S(1)}, bf16[2048]{0:T(1024)(128)(2,1)}, u32[]{:S(2)}) copy-start(bf16[2048]{0:T(1024)(128)(2,1)} %param.37) | copy-start | bytes 12292
  30.8 3.4 %collective-permute-start = (bf16[6,2048]{1,0:T(8,128)(2,1)S(1)}, bf16[6,2048]{1,0:T(8,128)(2,1)S(1)}, u32[]{:S(2)}, u32[]{:S(2)}) collective-permute-start(bf16[6,2048]{1,0:T(8,128)(2,1)S(1)} %slice.2), channel_id=1, source_target_pairs={{0,1},{1,2},{2,3},{4,5},{5,6},{6,7},{8,9},{9,10},{10,11},{12,13},{... | collective-permute-start | bytes 73736
  42.6 15.3 %all-to-all-start = ((bf16[8,7,2048]{2,1,0:T(8,128)(2,1)}), bf16[8,7,2048]{2,1,0:T(8,128)(2,1)S(1)}, u32[]{:S(2)}, u32[]{:S(2)}) async-start(bf16[8,7,2048]{2,1,0:T(8,128)(2,1)} %reshape.269), calls=%async_computation | async-start | bytes 524288 | tf_op jit(solution)/shard_map/all_to_all | solution.py:151
  63.3 12.6 %all-to-all-start.1 = ((bf16[8,7,2048]{2,1,0:T(8,128)(2,1)}), bf16[8,7,2048]{2,1,0:T(8,128)(2,1)S(1)}, u32[]{:S(2)}, u32[]{:S(2)}) async-start(bf16[8,7,2048]{2,1,0:T(8,128)(2,1)} %reshape.271), calls=%async_computation.1 | async-start | bytes 524288 | tf_op jit(solution)/shard_map/all_to_all | solution.py:155
